TPU v7x, 32 devices: a whole 2x2x4 slice. The times are simulated.
32 devices in a mesh: fs: 16 (over z, y, x), tp: 2 (over core).
Axes of the slice: x: 2, y: 2, z: 4, core: 2. Of those that a mesh axis runs over, the one named last changes fastest.
Arguments:
- inputs: bfloat16 [8192, 2048], P('fs', 'tp'), may hold values from -6 to 6
- hidden_pre: bfloat16 [8192, 4096], P('fs', 'tp'), may hold values from -6 to 6
- norm_input: bfloat16 [8192, 2048], P('fs', 'tp'), may hold values from -48 to 48, as said below
- out_gain: float32 [2048], P('tp'), may hold values from 0.1 to 1.9
- w_up: bfloat16 [2048, 4096], P('tp', 'fs'), may hold values from -0.125 to 0.125
- w_down: bfloat16 [4096, 2048], P('tp', 'fs'), may hold values from -0.09375 to 0.09375
- cotangent: bfloat16 [8192, 2048], P('fs', 'tp'), may hold values from -6 to 6
Outputs:
- grad_input: bfloat16 [8192, 2048], P('fs', 'tp')
- grad_up: float32 [2048, 4096], P('tp', 'fs')
- grad_gain: float32 [2048], P('tp')
Inputs may be any that keep to these rules, and one draw needn't show every extreme that they name: `norm_input`: each token's features are scaled by a factor of that token, and each block of 2048 / 2 features by a factor of that block.
All inputs are finite; a program needn't handle non-finite values.
Results may differ from a plain program's by a relative error of at most 0.0058.
Values may be sent and summed in bfloat16 or wider, within the bound.
A program may use at most 64 MiB of HBM per device.

v0:
```python
import jax
import jax.numpy as jnp
from jax import lax
from jax.sharding import PartitionSpec as P

norm_eps = 1e-06


def on_device(inputs, hidden_pre, norm_input, out_gain, w_up, w_down, cotangent):
    tok_rows = inputs.shape[0]
    width = inputs.shape[1] * lax.axis_size("tp")
    scaled = (tok_rows * lax.axis_size("fs")) ** (-0.5)
    normed = norm_input.astype(jnp.float32)
    upstream = cotangent.astype(jnp.float32)
    weighted = upstream * out_gain
    square_sum, cross_sum = lax.psum(
        (jnp.sum(normed * normed, axis=1), jnp.sum(weighted * normed, axis=1)), "tp"
    )
    inv_rms = lax.rsqrt(square_sum / width + norm_eps)[:, None]
    cross_mean = (cross_sum / width)[:, None]
    d_out = (weighted * inv_rms - normed * inv_rms * inv_rms * inv_rms * cross_mean).astype(
        jnp.bfloat16
    )
    grad_gain = lax.psum(jnp.sum(upstream * normed * inv_rms, axis=0) * scaled, "fs")
    out_full = lax.all_gather(d_out, "tp", axis=1, tiled=True)
    columns = out_full
    d_act = lax.dot_general(
        columns,
        lax.all_gather(w_down, "fs", axis=1, tiled=True),
        (((1,), (1,)), ((), ())),
        preferred_element_type=jnp.float32,
    )
    d_pre = (d_act * 2.0 * jax.nn.relu(hidden_pre.astype(jnp.float32))).astype(jnp.bfloat16)
    hidden_full = lax.all_gather(d_pre, "tp", axis=1, tiled=True)
    columns = hidden_full
    grad_input = lax.dot_general(
        columns,
        lax.all_gather(w_up, "fs", axis=1, tiled=True),
        (((1,), (1,)), ((), ())),
        preferred_element_type=jnp.float32,
    ).astype(jnp.bfloat16)
    columns = hidden_full
    grad_up = lax.psum_scatter(
        lax.dot_general(
            columns, inputs, (((0,), (0,)), ((), ())), preferred_element_type=jnp.float32
        )
        * scaled,
        "fs",
        scatter_dimension=0,
        tiled=True,
    ).T
    return (grad_input, grad_up, grad_gain)


def solution(mesh):
    placed = (
        P("fs", "tp"),
        P("fs", "tp"),
        P("fs", "tp"),
        P("tp"),
        P("tp", "fs"),
        P("tp", "fs"),
        P("fs", "tp"),
    )
    return jax.shard_map(
        on_device,
        mesh=mesh,
        in_specs=placed,
        out_specs=(P("fs", "tp"), P("tp", "fs"), P("tp")),
        check_vma=False,
    )
```

profile of v0, /device:TPU:10, one launch (start us, length us, event | category | flops | bytes accessed | tf_op | source)
XLA Modules:
  0.0 698.5 jit_solution(14168805298749167662)
XLA Ops:
  7.2 0.0 copy-start
  7.2 0.0 copy-start.1
  7.2 0.0 copy-start.2
  7.2 0.0 copy-start.3
  7.2 0.0 all-gather.5.cloned.1.call-start
  7.3 1.7 fusion.3
  8.9 2.5 psum.21
  11.4 2.4 fusion.9
  13.8 2.5 psum.22
  16.3 0.0 copy-done.1
  16.3 0.0 copy-done.2
  16.3 0.0 copy-done.3
  16.3 1.7 fusion.2
  18.0 0.0 all-gather.5.cloned.1.call-update
  18.0 0.0 all-gather.7.cloned.1.call-start
  18.0 0.7 all-gather.7.cloned.1.call-update
  18.7 0.0 all-gather.9.cloned.1.call-start
  18.8 11.3 %all-gather.5.cloned.1.call-done = bf16[512,2048]{1,0:T(8,128)(2,1)} async-done(((bf16[512,1024]{1,0:T(8,128)(2,1)}), bf16[512,2048]{1,0:T(8,128)(2,1)}) %all-gather.5.cloned.1.call-update) | async-done | bytes 2097168 | tf_op jit(solution)/shard_map/all_gather | solution.py:25
  30.1 142.7 %all-gather.7.cloned.1.call-done = bf16[2048,2048]{1,0:T(8,128)(2,1)} async-done(((bf16[2048,128]{1,0:T(8,128)(2,1)}), bf16[2048,2048]{1,0:T(8,128)(2,1)}) %all-gather.7.cloned.1.call-update) | async-done | bytes 8388624 | tf_op jit(solution)/shard_map/all_gather | solution.py:29
  172.8 10.5 %multiply_convert_fusion = bf16[512,2048]{1,0:T(8,128)(2,1)} fusion(bf16[512,2048]{1,0:T(8,128)(2,1)} %param.8, bf16[512,2048]{1,0:T(8,128)(2,1)} %all-gather.5.cloned.1.call-done, bf16[2048,2048]{1,0:T(8,128)(2,1)} %all-gather.7.cloned.1.call-done), kind=kOutput, calls=%fused_computation.1 | convolution fusion | flops 4300210176 | bytes 14680064 | tf_op jit(solution)/shard_map/dot_general | solution.py:27
  183.3 0.0 all-gather.9.cloned.1.call-update
  183.3 0.0 all-gather.11.cloned.1.call-start
  183.4 0.5 all-gather.11.cloned.1.call-update
  183.9 0.0 reduce-scatter.2.cloned.1.call-start
  184.0 14.4 %all-gather.9.cloned.1.call-done = bf16[512,4096]{1,0:T(8,128)(2,1)} async-done(((bf16[512,2048]{1,0:T(8,128)(2,1)}), bf16[512,4096]{1,0:T(8,128)(2,1)}) %all-gather.9.cloned.1.call-update) | async-done | bytes 4194320 | tf_op jit(solution)/shard_map/all_gather | solution.py:34
  198.4 0.0 copy-done
  198.4 10.4 %broadcast_multiply_fusion = f32[4096,1024]{1,0:T(8,128)} fusion(bf16[512,4096]{1,0:T(8,128)(2,1)} %all-gather.9.cloned.1.call-done, bf16[512,1024]{1,0:T(8,128)(2,1)S(1)} %copy-done), kind=kOutput, calls=%fused_computation | convolution fusion | flops 4299161600 | bytes 22020096 | tf_op jit(solution)/shard_map/dot_general | solution.py:44
  208.8 0.0 reduce-scatter.2.cloned.1.call-update
  208.8 32.1 %psum.23 = f32[1024]{0:T(1024)} all-reduce(f32[1024]{0:T(1024)S(1)} %broadcast_multiply_fusion.1), channel_id=1, replica_groups=mesh['fs'=16,'tp'=2] {'fs'}, use_global_device_ids=true, to_apply=%region_6.7 | all-reduce | flops 1024 | bytes 8192 | tf_op jit(solution)/shard_map/psum | solution.py:24
  240.9 93.3 %all-gather.11.cloned.1.call-done = bf16[1024,4096]{1,0:T(8,128)(2,1)} async-done(((bf16[1024,256]{1,0:T(8,128)(2,1)}), bf16[1024,4096]{1,0:T(8,128)(2,1)}) %all-gather.11.cloned.1.call-update) | async-done | bytes 8388624 | tf_op jit(solution)/shard_map/all_gather | solution.py:38
  334.2 10.2 %convolution_convert_fusion = bf16[512,1024]{1,0:T(8,128)(2,1)} fusion(bf16[512,4096]{1,0:T(8,128)(2,1)} %all-gather.9.cloned.1.call-done, bf16[1024,4096]{1,0:T(8,128)(2,1)} %all-gather.11.cloned.1.call-done), kind=kOutput, calls=%fused_computation.17 | convolution fusion | flops 4295491584 | bytes 13631488 | tf_op jit(solution)/shard_map/dot_general | solution.py:36
  344.4 345.0 %reduce-scatter.2.cloned.1.call-done = f32[256,1024]{1,0:T(8,128)} async-done(((f32[4096,1024]{1,0:T(8,128)}), f32[256,1024]{1,0:T(8,128)}) %reduce-scatter.2.cloned.1.call-update) | async-done | bytes 1048592 | tf_op jit(solution)/shard_map/reduce_scatter | solution.py:43
  689.4 2.5 copy.10
  (3 shorter events, 0.0 us)
Async XLA Ops:
  7.2 191.2 %copy-start = (bf16[512,1024]{1,0:T(8,128)(2,1)S(1)}, bf16[512,1024]{1,0:T(8,128)(2,1)}, u32[]{:S(2)}) copy-start(bf16[512,1024]{1,0:T(8,128)(2,1)} %param.7) | copy-start | bytes 3145732
  7.2 9.1 %copy-start.1 = (bf16[512,1024]{1,0:T(8,128)(2,1)S(1)}, bf16[512,1024]{1,0:T(8,128)(2,1)}, u32[]{:S(2)}) copy-start(bf16[512,1024]{1,0:T(8,128)(2,1)} %param.9) | copy-start | bytes 3145732
  7.2 9.1 %copy-start.2 = (bf16[512,1024]{1,0:T(8,128)(2,1)S(1)}, bf16[512,1024]{1,0:T(8,128)(2,1)}, u32[]{:S(2)}) copy-start(bf16[512,1024]{1,0:T(8,128)(2,1)} %param.13) | copy-start | bytes 3145732
  7.2 9.1 %copy-start.3 = (f32[1024]{0:T(1024)S(1)}, f32[1024]{0:T(1024)}, u32[]{:S(2)}) copy-start(f32[1024]{0:T(1024)} %param.10) | copy-start | bytes 12292
  7.2 22.9 %all-gather.5.cloned.1.call-start = ((), (), s32[]{:S(2)}) async-start(), calls=%async_computation.1 | async-start | bytes 3145728 | tf_op jit(solution)/shard_map/all_gather | solution.py:25
  18.0 154.8 %all-gather.7.cloned.1.call-start = ((), (), s32[]{:S(2)}) async-start(), calls=%async_computation.2 | async-start | bytes 8912896 | tf_op jit(solution)/shard_map/all_gather | solution.py:29
  18.7 179.7 %all-gather.9.cloned.1.call-start = ((), (), s32[]{:S(2)}) async-start(), calls=%async_computation.3 | async-start | bytes 6291456 | tf_op jit(solution)/shard_map/all_gather | solution.py:34
  183.3 150.9 %all-gather.11.cloned.1.call-start = ((), (), s32[]{:S(2)}) async-start(), calls=%async_computation.4 | async-start | bytes 8912896 | tf_op jit(solution)/shard_map/all_gather | solution.py:38
  183.9 505.5 %reduce-scatter.2.cloned.1.call-start = ((), (), s32[]{:S(2)}) async-start(), calls=%async_computation.5 | async-start | bytes 17825792 | tf_op jit(solution)/shard_map/reduce_scatter | solution.py:43
Sparse Core Ops, SparseCore 0:
  18.1 11.9 all-gather.4
  32.8 139.9 all-gather.6
  183.5 14.8 all-gather.8
  201.0 133.2 all-gather.10
  336.4 352.9 reduce-scatter.1
where the time goes:
time: 699 us; the launch traced here: 698 us
  waiting for transfers between devices  608 us (87%)
  blocking collectives  37.1 us (5%)
  matrix products  31 us (4%)
  between operations  13.8 us (2%)
    reduce_scatter x1, waiting for transfers between devices, on_device(): lax.psum_scatter(lax.dot_general(columns, inputs, (((0,), (0,)), ((), ())...  345 us
    all_gather x1, waiting for transfers between devices, on_device(): lax.all_gather(w_down, 'fs', axis=1, tiled=True)  143 us
    all_gather x1, waiting for transfers between devices, on_device(): lax.all_gather(w_up, 'fs', axis=1, tiled=True)  93.3 us
    psum x1, blocking collectives, on_device(): lax.psum(jnp.sum(upstream * normed * inv_rms, axis=0) * scaled, 'fs')  32.1 us
    all_gather x1, waiting for transfers between devices, on_device(): hidden_full = lax.all_gather(d_pre, 'tp', axis=1, tiled=True)  14.4 us
  transfers between devices with their start and end apart: 5, of which 5 were waited for; matrix products, arithmetic and copies ran while one was open for 3% of the time, Pallas kernels for 0%

commit v1 on v0

--- a/solution.py
+++ b/solution.py
@@ -24,11 +24,9 @@
     grad_gain = lax.psum(jnp.sum(upstream * normed * inv_rms, axis=0) * scaled, "fs")
     out_full = lax.all_gather(d_out, "tp", axis=1, tiled=True)
     columns = out_full
+    ends_drive = lambda sheet: jnp.concatenate(lax.all_gather(sheet, axis_name="fs"), 1)
     d_act = lax.dot_general(
-        columns,
-        lax.all_gather(w_down, "fs", axis=1, tiled=True),
-        (((1,), (1,)), ((), ())),
-        preferred_element_type=jnp.float32,
+        columns, ends_drive(w_down), (((1,), (1,)), ((), ())), preferred_element_type=jnp.float32
     )
     d_pre = (d_act * 2.0 * jax.nn.relu(hidden_pre.astype(jnp.float32))).astype(jnp.bfloat16)
     hidden_full = lax.all_gather(d_pre, "tp", axis=1, tiled=True)

time: 699 us -> 661 us (0.946)
  waiting for transfers between devices: 608 us -> 559 us
  local copies, waits for them, and re-layouts: 2.56 us -> 15.1 us
    all_gather x1, waiting for transfers between devices: 143 us -> 105 us  [on_device(): lax.all_gather(sheet, axis_name='fs')]
    reshape x0 -> x1, local copies, waits for them, and re-layouts: none -> 12.6 us  [on_device(): jnp.concatenate(lax.all_gather(sheet, axis_name='fs'), 1)]
    all_gather x1, waiting for transfers between devices: 11.3 us -> 0.01 us  [on_device(): out_full = lax.all_gather(d_out, 'tp', axis=1, tiled=True)]
  transfers between devices with their start and end apart: 5 -> 5, of which waited for: 5 -> 4; matrix products, arithmetic and copies ran while one was open for 3% -> 6% of each run, Pallas kernels for 0% -> 0%
where the time goes in v1:
time: 661 us; the launch traced here: 660 us
  waiting for transfers between devices  559 us (85%)
  blocking collectives  37 us (6%)
  matrix products  30.4 us (5%)
  local copies, waits for them, and re-layouts  15.1 us (2%)
  between operations  13.8 us (2%)
    reduce_scatter x1, waiting for transfers between devices, on_device(): lax.psum_scatter(lax.dot_general(columns, inputs, (((0,), (0,)), ((), ())...  345 us
    all_gather x1, waiting for transfers between devices, on_device(): lax.all_gather(sheet, axis_name='fs')  105 us
    all_gather x1, waiting for transfers between devices, on_device(): lax.all_gather(w_up, 'fs', axis=1, tiled=True)  93.4 us
    psum x1, blocking collectives, on_device(): lax.psum(jnp.sum(upstream * normed * inv_rms, axis=0) * scaled, 'fs')  32 us
    all_gather x1, waiting for transfers between devices, on_device(): hidden_full = lax.all_gather(d_pre, 'tp', axis=1, tiled=True)  14.1 us
  transfers between devices with their start and end apart: 5, of which 4 were waited for; matrix products, arithmetic and copies ran while one was open for 6% of the time, Pallas kernels for 0%

profile of v1, /device:TPU:10, one launch (start us, length us, event | category | flops | bytes accessed | tf_op | source)
XLA Modules:
  0.0 660.5 jit_solution(6248854844904841484)
XLA Ops:
  7.2 0.0 copy-start
  7.2 0.0 copy-start.1
  7.2 0.0 copy-start.2
  7.2 0.0 copy-start.3
  7.2 0.0 all-gather.12.cloned.1.call-start
  7.3 0.7 all-gather.12.cloned.1.call-update
  7.9 0.0 all-gather.6.cloned.1.call-start
  8.0 1.5 fusion.3
  9.5 2.5 psum.21
  12.0 0.0 copy-done.1
  12.0 2.1 fusion.9
  14.1 2.5 psum.22
  16.6 0.0 copy-done.2
  16.6 0.0 copy-done.3
  16.6 1.7 fusion.2
  18.2 0.0 all-gather.6.cloned.1.call-update
  18.3 0.0 all-gather.8.cloned.1.call-start
  18.3 104.8 %all-gather.12.cloned.1.call-done = bf16[32768,128]{1,0:T(8,128)(2,1)} async-done(((bf16[2048,128]{1,0:T(8,128)(2,1)}), bf16[32768,128]{1,0:T(8,128)(2,1)}) %all-gather.12.cloned.1.call-update) | async-done | bytes 8388624 | tf_op jit(solution)/shard_map/all_gather | solution.py:27
  123.1 0.0 copy-start.4
  123.1 12.6 %copy.12 = bf16[2048,16,128]{0,2,1:T(8,128)(2,1)} copy(bf16[2048,16,128]{2,0,1:T(8,128)(2,1)} %bitcast.11) | data formatting | bytes 16777216 | tf_op jit(solution)/shard_map/reshape | solution.py:27
  135.7 0.0 all-gather.6.cloned.1.call-done
  135.7 0.0 copy-done.4
  135.7 9.9 %multiply_convert_fusion = bf16[512,2048]{1,0:T(8,128)(2,1)} fusion(bf16[512,2048]{1,0:T(8,128)(2,1)S(1)} %copy-done.4, bf16[512,2048]{1,0:T(8,128)(2,1)} %all-gather.6.cloned.1.call-done, bf16[2048,2048]{0,1:T(8,128)(2,1)} %bitcast.12), kind=kOutput, calls=%fused_computation.1 | convolution fusion | flops 4300210176 | bytes 14680064 | tf_op jit(solution)/shard_map/dot_general | solution.py:28
  145.7 0.0 all-gather.8.cloned.1.call-update
  145.7 0.0 all-gather.10.cloned.1.call-start
  145.8 0.5 all-gather.10.cloned.1.call-update
  146.3 0.0 reduce-scatter.2.cloned.1.call-start
  146.3 14.1 %all-gather.8.cloned.1.call-done = bf16[512,4096]{1,0:T(8,128)(2,1)} async-done(((bf16[512,2048]{1,0:T(8,128)(2,1)}), bf16[512,4096]{1,0:T(8,128)(2,1)}) %all-gather.8.cloned.1.call-update) | async-done | bytes 4194320 | tf_op jit(solution)/shard_map/all_gather | solution.py:32
  160.4 0.0 copy-done
  160.4 10.3 %broadcast_multiply_fusion = f32[4096,1024]{1,0:T(8,128)} fusion(bf16[512,4096]{1,0:T(8,128)(2,1)} %all-gather.8.cloned.1.call-done, bf16[512,1024]{1,0:T(8,128)(2,1)S(1)} %copy-done), kind=kOutput, calls=%fused_computation | convolution fusion | flops 4299161600 | bytes 22020096 | tf_op jit(solution)/shard_map/dot_general | solution.py:42
  170.7 0.0 reduce-scatter.2.cloned.1.call-update
  170.8 32.0 %psum.23 = f32[1024]{0:T(1024)} all-reduce(f32[1024]{0:T(1024)S(1)} %broadcast_multiply_fusion.1), channel_id=1, replica_groups=mesh['fs'=16,'tp'=2] {'fs'}, use_global_device_ids=true, to_apply=%region_6.7 | all-reduce | flops 1024 | bytes 8192 | tf_op jit(solution)/shard_map/psum | solution.py:24
  202.8 93.4 %all-gather.10.cloned.1.call-done = bf16[1024,4096]{1,0:T(8,128)(2,1)} async-done(((bf16[1024,256]{1,0:T(8,128)(2,1)}), bf16[1024,4096]{1,0:T(8,128)(2,1)}) %all-gather.10.cloned.1.call-update) | async-done | bytes 8388624 | tf_op jit(solution)/shard_map/all_gather | solution.py:36
  296.2 10.1 %convolution_convert_fusion = bf16[512,1024]{1,0:T(8,128)(2,1)} fusion(bf16[512,4096]{1,0:T(8,128)(2,1)} %all-gather.8.cloned.1.call-done, bf16[1024,4096]{1,0:T(8,128)(2,1)} %all-gather.10.cloned.1.call-done), kind=kOutput, calls=%fused_computation.17 | convolution fusion | flops 4295491584 | bytes 13631488 | tf_op jit(solution)/shard_map/dot_general | solution.py:34
  306.4 345.0 %reduce-scatter.2.cloned.1.call-done = f32[256,1024]{1,0:T(8,128)} async-done(((f32[4096,1024]{1,0:T(8,128)}), f32[256,1024]{1,0:T(8,128)}) %reduce-scatter.2.cloned.1.call-update) | async-done | bytes 1048592 | tf_op jit(solution)/shard_map/reduce_scatter | solution.py:41
  651.4 2.5 copy.13
  (3 shorter events, 0.0 us)
Async XLA Ops:
  7.2 153.2 %copy-start = (bf16[512,1024]{1,0:T(8,128)(2,1)S(1)}, bf16[512,1024]{1,0:T(8,128)(2,1)}, u32[]{:S(2)}) copy-start(bf16[512,1024]{1,0:T(8,128)(2,1)} %param.7) | copy-start | bytes 3145732
  7.2 4.8 copy-start.1
  7.2 9.4 %copy-start.2 = (bf16[512,1024]{1,0:T(8,128)(2,1)S(1)}, bf16[512,1024]{1,0:T(8,128)(2,1)}, u32[]{:S(2)}) copy-start(bf16[512,1024]{1,0:T(8,128)(2,1)} %param.13) | copy-start | bytes 3145732
  7.2 9.4 %copy-start.3 = (f32[1024]{0:T(1024)S(1)}, f32[1024]{0:T(1024)}, u32[]{:S(2)}) copy-start(f32[1024]{0:T(1024)} %param.10) | copy-start | bytes 12292
  7.2 115.9 %all-gather.12.cloned.1.call-start = ((), (), s32[]{:S(2)}) async-start(), calls=%async_computation.5 | async-start | bytes 8912896 | tf_op jit(solution)/shard_map/all_gather | solution.py:27
  7.9 127.8 %all-gather.6.cloned.1.call-start = ((), (), s32[]{:S(2)}) async-start(), calls=%async_computation.1 | async-start | bytes 3145728 | tf_op jit(solution)/shard_map/all_gather | solution.py:25
  18.3 142.1 %all-gather.8.cloned.1.call-start = ((), (), s32[]{:S(2)}) async-start(), calls=%async_computation.2 | async-start | bytes 6291456 | tf_op jit(solution)/shard_map/all_gather | solution.py:32
  123.1 12.6 %copy-start.4 = (bf16[512,2048]{1,0:T(8,128)(2,1)S(1)}, bf16[512,2048]{1,0:T(8,128)(2,1)}, u32[]{:S(2)}) copy-start(bf16[512,2048]{1,0:T(8,128)(2,1)} %param.8) | copy-start | bytes 6291460
  145.7 150.5 %all-gather.10.cloned.1.call-start = ((), (), s32[]{:S(2)}) async-start(), calls=%async_computation.3 | async-start | bytes 8912896 | tf_op jit(solution)/shard_map/all_gather | solution.py:36
  146.3 505.1 %reduce-scatter.2.cloned.1.call-start = ((), (), s32[]{:S(2)}) async-start(), calls=%async_computation.4 | async-start | bytes 17825792 | tf_op jit(solution)/shard_map/reduce_scatter | solution.py:41
Sparse Core Ops, SparseCore 0:
  10.8 112.3 all-gather.11
  125.3 10.1 all-gather.5
  145.8 14.5 all-gather.7
  163.0 133.2 all-gather.9
  298.4 352.9 reduce-scatter.1
